TPU v7x, 32 devices: a whole 2x2x4 slice. The times are simulated.
32 devices in a mesh: grp: 2 (over x), sp: 8 (over z, y), tp: 2 (over core).
Axes of the slice: x: 2, y: 2, z: 4, core: 2. Of those that a mesh axis runs over, the one named last changes fastest.
Arguments:
- resid: bfloat16 [2048, 2048], P(('grp', 'sp')), parts along dimension 0, may hold values from -6 to 6
- queries_first: bfloat16 [2048, 2048], P(('grp', 'sp'), 'tp'), parts along dimension 0, may hold values from -150 to 150
- keys_first: bfloat16 [2048, 2048], P(('grp', 'sp'), 'tp'), parts along dimension 0, may hold values from -6 to 6
- values_first: bfloat16 [2048, 2048], P(('grp', 'sp'), 'tp'), parts along dimension 0, may hold values from -6 to 6
- rel_first: float32 [16, 257], P('tp'), may hold values from -4 to 4
- post_first: float32 [2048], replicated, may hold values from 0.1 to 1.9
- out_first: bfloat16 [2048, 2048], P('tp', 'sp'), may hold values from -0.125 to 0.125
- pre_second: float32 [2048], replicated, may hold values from 0.1 to 1.9
- query_weight: bfloat16 [2048, 2048], P('sp', 'tp'), may hold values from -0.125 to 0.125
- key_weight: bfloat16 [2048, 2048], P('sp', 'tp'), may hold values from -0.125 to 0.125
- value_weight: bfloat16 [2048, 2048], P('sp', 'tp'), may hold values from -0.125 to 0.125
- rel_second: float32 [16, 257], P('tp'), may hold values from -4 to 4
- post_second: float32 [2048], replicated, may hold values from 0.1 to 1.9
- out_second: bfloat16 [2048, 2048], P('tp', 'sp'), may hold values from -0.125 to 0.125
Outputs:
- hidden_two: bfloat16 [2048, 2048], P(('grp', 'sp')), parts along dimension 0
There are 2 independent parts, one for each index of `grp`. A program takes and returns all parts, laid end to end along the dimension named above; an argument that names none is the same for every part. Nothing has to cross between parts.
All inputs are finite; a program needn't handle non-finite values.
Results may differ from a plain program's by a relative error of at most 0.017.
Values may be sent and summed in bfloat16 or wider, within the bound.
A program may use at most 128 MiB of HBM per device.

v0:
```python
import jax
import jax.numpy as jnp
from jax import lax
from jax.sharding import PartitionSpec as P

SEG = 64
LEFT = 8
REACH = 512
REL_CLIP = 128


EPS = 1e-06
NEG_FILL = -1e30


def from_behind(value, axis, steps):
    count = lax.axis_size(axis)
    initial, last = (max(0, -steps), min(count, count - steps))
    return lax.ppermute(value, axis, [(source, source + steps) for source in range(initial, last)])


def band_bias(bias_table):
    heads_here = bias_table.shape[0]
    band = (LEFT + 1) * SEG
    length = SEG + band
    index = jnp.arange(length, dtype=jnp.int32)
    distance = jnp.where(index < band, LEFT * SEG - index, LEFT * SEG + length - index)
    slot = jnp.clip(distance, -REL_CLIP, REL_CLIP) + REL_CLIP
    onehot = (slot[:, None] == jnp.arange(2 * REL_CLIP + 1, dtype=jnp.int32)[None, :]).astype(
        jnp.float32
    )
    diagonal_values = jnp.dot(bias_table, onehot.T, precision=lax.Precision.HIGHEST)
    spread = jnp.broadcast_to(diagonal_values[:, None, :], (heads_here, SEG, length)).reshape(
        heads_here, SEG * length
    )
    return spread[:, : SEG * (length - 1)].reshape(heads_here, SEG, length - 1)[:, :, :band]


def attend_band(queries, key_rows, value_rows, bias, key_live):
    rows, width = queries.shape
    heads_here = bias.shape[0]
    head_size = width // heads_here
    blocks = rows // SEG
    query_seg = queries.reshape(blocks, SEG, heads_here, head_size)
    key_seg = key_rows.reshape(blocks + LEFT, SEG, heads_here, head_size)
    value_seg = value_rows.reshape(blocks + LEFT, SEG, heads_here, head_size)
    live_seg = key_live.reshape(blocks + LEFT, SEG)
    key_band = jnp.concatenate(
        [key_seg[earlier : earlier + blocks] for earlier in range(LEFT + 1)], axis=1
    )
    value_band = jnp.concatenate(
        [value_seg[earlier : earlier + blocks] for earlier in range(LEFT + 1)], axis=1
    )
    live_band = jnp.concatenate(
        [live_seg[earlier : earlier + blocks] for earlier in range(LEFT + 1)], axis=1
    )
    scores = jnp.einsum("nqhd,nkhd->nhqk", query_seg, key_band, preferred_element_type=jnp.float32)
    scores = scores * head_size ** (-0.5) + bias[None]
    scores = jnp.where(live_band[:, None, None, :], scores, NEG_FILL)
    largest = jnp.max(scores, axis=-1, keepdims=True)
    weights = jnp.exp(scores - largest)
    weights = (weights / jnp.sum(weights, axis=-1, keepdims=True)).astype(jnp.bfloat16)
    mixed = jnp.einsum("nhqk,nkhd->nqhd", weights, value_band, preferred_element_type=jnp.float32)
    return mixed.astype(jnp.bfloat16).reshape(rows, width)


def extend_rows(pieces, member, own_rows):
    joined = jnp.concatenate([piece[member] for piece in pieces] + [own_rows], axis=0)
    return joined


def normed(hidden, gain):
    values = hidden.astype(jnp.float32)
    scale = lax.rsqrt(jnp.mean(values * values, axis=-1, keepdims=True) + EPS)
    return (values * scale * gain).astype(jnp.bfloat16)


def residual_add(branch, residual, gain):
    values = branch.astype(jnp.float32)
    scale = lax.rsqrt(jnp.mean(values * values, axis=-1, keepdims=True) + EPS)
    return (residual.astype(jnp.float32) + values * scale * gain).astype(jnp.bfloat16)


def combine(mixed, weight, residual, gain):
    partial_rows = jnp.dot(
        mixed, lax.all_gather(weight, "sp", axis=1, tiled=True), preferred_element_type=jnp.float32
    )
    branch = lax.psum_scatter(
        partial_rows.astype(jnp.bfloat16), "tp", scatter_dimension=0, tiled=True
    )
    return residual_add(branch, residual, gain)


def full_rows(share):
    return lax.all_gather(share, "tp", axis=0, tiled=True)


def shards(
    resid,
    queries_first,
    keys_first,
    values_first,
    rel_first,
    post_first,
    out_first,
    pre_second,
    query_weight,
    key_weight,
    value_weight,
    rel_second,
    post_second,
    out_second,
):
    tok_rows = resid.shape[0]
    depth = (REACH + tok_rows - 1) // tok_rows
    anchor = lax.axis_index("sp") * tok_rows
    key_live = anchor - REACH + jnp.arange(tok_rows + REACH, dtype=jnp.int32) >= 0
    share_rows = tok_rows // lax.axis_size("tp")
    base_rows = lax.dynamic_slice_in_dim(resid, lax.axis_index("tp") * share_rows, share_rows, 0)
    earlier_first = [
        from_behind((keys_first, values_first), "sp", distance) for distance in range(depth, 0, -1)
    ]
    key_ext = extend_rows(earlier_first, 0, keys_first)
    value_ext = extend_rows(earlier_first, 1, values_first)
    first = attend_band(queries_first, key_ext, value_ext, band_bias(rel_first), key_live)
    hidden_one = combine(first, out_first, base_rows, post_first)
    inputs_two = full_rows(normed(hidden_one, pre_second))
    query_sum = jnp.dot(
        inputs_two,
        lax.all_gather(query_weight, "sp", axis=0, tiled=True),
        preferred_element_type=jnp.float32,
    )
    key_sum = jnp.dot(
        inputs_two,
        lax.all_gather(key_weight, "sp", axis=0, tiled=True),
        preferred_element_type=jnp.float32,
    )
    value_sum = jnp.dot(
        inputs_two,
        lax.all_gather(value_weight, "sp", axis=0, tiled=True),
        preferred_element_type=jnp.float32,
    )
    queries_two = query_sum.astype(jnp.bfloat16)
    keys_two = key_sum.astype(jnp.bfloat16)
    values_two = value_sum.astype(jnp.bfloat16)
    earlier_second = [
        from_behind((keys_two, values_two), "sp", distance) for distance in range(depth, 0, -1)
    ]
    key_ext_two = extend_rows(earlier_second, 0, keys_two)
    value_ext_two = extend_rows(earlier_second, 1, values_two)
    second = attend_band(queries_two, key_ext_two, value_ext_two, band_bias(rel_second), key_live)
    hidden_two = combine(second, out_second, hidden_one, post_second)
    return full_rows(hidden_two)


def solution(mesh):
    in_specs = (
        P(("grp", "sp"), None),
        P(("grp", "sp"), "tp"),
        P(("grp", "sp"), "tp"),
        P(("grp", "sp"), "tp"),
        P("tp", None),
        P(),
        P("tp", "sp"),
        P(),
        P("sp", "tp"),
        P("sp", "tp"),
        P("sp", "tp"),
        P("tp", None),
        P(),
        P("tp", "sp"),
    )
    out_specs = P(("grp", "sp"), None)
    return jax.shard_map(shards, mesh=mesh, in_specs=in_specs, out_specs=out_specs, check_vma=False)
```

profile of v0, /device:TPU:29, one launch (start us, length us, event | category | flops | bytes accessed | tf_op | source)
XLA Modules:
  0.0 517.0 jit_solution(16350053045093541963)
XLA Ops:
  6.5 0.7 all-gather.6.cloned.1.call-update
  7.3 1.3 collective-permute-start.4
  8.6 1.3 collective-permute-start.5
  9.9 1.3 collective-permute-start.6
  11.2 1.3 collective-permute-start.7
  12.5 1.3 collective-permute-start
  13.8 0.6 convolution_bitcast_fusion.1
  14.5 1.7 copy.83
  16.3 2.4 reshape.142
  18.7 1.0 copy.84
  19.7 0.8 copy.93
  20.5 18.3 %collective-permute-done.4 = bf16[128,1024]{1,0:T(8,128)(2,1)S(1)} collective-permute-done((bf16[128,1024]{1,0:T(8,128)(2,1)}, bf16[128,1024]{1,0:T(8,128)(2,1)S(1)}, u32[]{:S(2)}, u32[]{:S(2)}) %collective-permute-start.4) | collective-permute-done | bytes 262176 | tf_op jit(solution)/shard_map/ppermute | solution.py:19
  38.8 1.3 collective-permute-start.1
  40.1 1.3 collective-permute-start.2
  41.4 1.3 collective-permute-start.3
  42.7 0.1 concatenate.73
  43.3 62.5 %collective-permute-done = bf16[128,1024]{1,0:T(8,128)(2,1)S(1)} collective-permute-done((bf16[128,1024]{1,0:T(8,128)(2,1)}, bf16[128,1024]{1,0:T(8,128)(2,1)S(1)}, u32[]{:S(2)}, u32[]{:S(2)}) %collective-permute-start) | collective-permute-done | bytes 262176 | tf_op jit(solution)/shard_map/ppermute | solution.py:19
  107.1 0.3 copy-done.5
  108.2 1.5 copy-done.7
  109.6 2.5 fusion.55
  112.1 2.5 fusion.88
  114.6 4.9 fusion.19
  119.5 0.2 copy.54
  119.7 3.2 all-gather.6.cloned.1.call-done
  122.9 3.7 convolution_convert_fusion.1
  126.6 0.7 all-gather.12.cloned.1.call-update
  127.4 0.5 all-gather.8.cloned.1.call-update
  128.0 0.5 all-gather.10.cloned.1.call-update
  128.5 0.5 all-gather.14.cloned.1.call-update
  129.2 0.6 convolution_bitcast_fusion
  129.9 2.4 reshape.146
  132.3 24.8 %reduce-scatter.3.cloned.1.call-done = bf16[64,2048]{1,0:T(8,128)(2,1)} async-done(((bf16[128,2048]{1,0:T(8,128)(2,1)}), bf16[64,2048]{1,0:T(8,128)(2,1)}) %reduce-scatter.3.cloned.1.call-update) | async-done | bytes 262160 | tf_op jit(solution)/shard_map/reduce_scatter | solution.py:88
  157.0 1.1 fusion.21
  158.2 1.3 fusion.27
  159.5 0.1 fusion.29
  159.6 2.4 all_gather.22
  162.0 68.0 %all-gather.12.cloned.1.call-done = bf16[2048,1024]{1,0:T(8,128)(2,1)} async-done(((bf16[256,1024]{1,0:T(8,128)(2,1)}), bf16[2048,1024]{1,0:T(8,128)(2,1)}) %all-gather.12.cloned.1.call-update) | async-done | bytes 4194320 | tf_op jit(solution)/shard_map/all_gather | solution.py:135
  230.0 2.9 convolution_convert_fusion.2
  232.9 1.3 collective-permute-start.12
  234.2 1.3 collective-permute-start.13
  235.5 1.3 collective-permute-start.14
  236.8 1.3 collective-permute-start.15
  238.1 84.8 %all-gather.8.cloned.1.call-done = bf16[2048,1024]{1,0:T(8,128)(2,1)} async-done(((bf16[256,1024]{1,0:T(8,128)(2,1)}), bf16[2048,1024]{1,0:T(8,128)(2,1)}) %all-gather.8.cloned.1.call-update) | async-done | bytes 4194320 | tf_op jit(solution)/shard_map/all_gather | solution.py:140
  323.0 2.9 convolution_convert_fusion.4
  325.9 1.3 collective-permute-start.10
  327.2 1.3 collective-permute-start.11
  328.6 1.3 collective-permute-start.8
  329.9 1.3 collective-permute-start.9
  331.2 85.5 %all-gather.10.cloned.1.call-done = bf16[2048,1024]{1,0:T(8,128)(2,1)} async-done(((bf16[256,1024]{1,0:T(8,128)(2,1)}), bf16[2048,1024]{1,0:T(8,128)(2,1)}) %all-gather.10.cloned.1.call-update) | async-done | bytes 4194320 | tf_op jit(solution)/shard_map/all_gather | solution.py:130
  416.7 2.9 fusion.18
  420.4 1.1 fusion.37
  421.6 1.0 copy.107
  424.3 1.5 copy-done.8
  425.7 2.5 fusion.53
  428.2 2.5 fusion.91
  430.8 4.9 fusion.20
  435.6 0.2 copy.74
  435.8 55.6 %all-gather.14.cloned.1.call-done = bf16[1024,2048]{1,0:T(8,128)(2,1)} async-done(((bf16[1024,256]{1,0:T(8,128)(2,1)}), bf16[1024,2048]{1,0:T(8,128)(2,1)}) %all-gather.14.cloned.1.call-update) | async-done | bytes 4194320 | tf_op jit(solution)/shard_map/all_gather | solution.py:86
  491.4 3.7 convolution_convert_fusion
  495.2 9.7 %reduce-scatter.5.cloned.1.call-done = bf16[64,2048]{1,0:T(8,128)(2,1)} async-done(((bf16[128,2048]{1,0:T(8,128)(2,1)}), bf16[64,2048]{1,0:T(8,128)(2,1)}) %reduce-scatter.5.cloned.1.call-update) | async-done | bytes 262160 | tf_op jit(solution)/shard_map/reduce_scatter | solution.py:88
  504.9 1.1 fusion.25
  506.0 1.1 fusion.30
  507.2 2.2 all_gather.27
  509.4 0.8 copy.208
  (127 shorter events, 5.0 us)
Async XLA Ops:
  6.5 7.3 %copy-start = (f32[8,257]{1,0:T(8,128)S(1)}, f32[8,257]{1,0:T(8,128)}, u32[]{:S(2)}) copy-start(f32[8,257]{1,0:T(8,128)} %param.18) | copy-start | bytes 24676
  6.5 116.3 %all-gather.6.cloned.1.call-start = ((), (), s32[]{:S(2)}) async-start(), calls=%async_computation.2 | async-start | bytes 4718592 | tf_op jit(solution)/shard_map/all_gather | solution.py:86
  7.3 149.8 %reduce-scatter.3.cloned.1.call-start = ((), (), s32[]{:S(2)}) async-start(), calls=%async_computation.3 | async-start | bytes 786432 | tf_op jit(solution)/shard_map/reduce_scatter | solution.py:88
  7.3 31.5 %collective-permute-start.4 = (bf16[128,1024]{1,0:T(8,128)(2,1)}, bf16[128,1024]{1,0:T(8,128)(2,1)S(1)}, u32[]{:S(2)}, u32[]{:S(2)}) collective-permute-start(bf16[128,1024]{1,0:T(8,128)(2,1)} %param.16), channel_id=1, source_target_pairs={{0,8},{2,10},{4,12},{6,14},{1,9},{3,11},{5,13},{7,15},{16,24},{18,... | collective-permute-start | bytes 786440 | tf_op jit(solution)/shard_map/ppermute | solution.py:19
  8.6 31.5 %collective-permute-start.5 = (bf16[128,1024]{1,0:T(8,128)(2,1)}, bf16[128,1024]{1,0:T(8,128)(2,1)S(1)}, u32[]{:S(2)}, u32[]{:S(2)}) collective-permute-start(bf16[128,1024]{1,0:T(8,128)(2,1)} %param.16), channel_id=1, source_target_pairs={{0,6},{2,8},{4,10},{6,12},{8,14},{1,7},{3,9},{5,11},{7,13},{9,15},... | collective-permute-start | bytes 786440 | tf_op jit(solution)/shard_map/ppermute | solution.py:19
  9.9 31.5 %collective-permute-start.6 = (bf16[128,1024]{1,0:T(8,128)(2,1)}, bf16[128,1024]{1,0:T(8,128)(2,1)S(1)}, u32[]{:S(2)}, u32[]{:S(2)}) collective-permute-start(bf16[128,1024]{1,0:T(8,128)(2,1)} %param.16), channel_id=1, source_target_pairs={{0,4},{2,6},{4,8},{6,10},{8,12},{10,14},{1,5},{3,7},{5,9},{7,11},{... | collective-permute-start | bytes 786440 | tf_op jit(solution)/shard_map/ppermute | solution.py:19
  11.2 31.6 %collective-permute-start.7 = (bf16[128,1024]{1,0:T(8,128)(2,1)}, bf16[128,1024]{1,0:T(8,128)(2,1)S(1)}, u32[]{:S(2)}, u32[]{:S(2)}) collective-permute-start(bf16[128,1024]{1,0:T(8,128)(2,1)} %param.16), channel_id=1, source_target_pairs={{0,2},{2,4},{4,6},{6,8},{8,10},{10,12},{12,14},{1,3},{3,5},{5,7},{... | collective-permute-start | bytes 786440 | tf_op jit(solution)/shard_map/ppermute | solution.py:19
  12.5 93.4 %collective-permute-start = (bf16[128,1024]{1,0:T(8,128)(2,1)}, bf16[128,1024]{1,0:T(8,128)(2,1)S(1)}, u32[]{:S(2)}, u32[]{:S(2)}) collective-permute-start(bf16[128,1024]{1,0:T(8,128)(2,1)} %param.17), channel_id=1, source_target_pairs={{0,8},{2,10},{4,12},{6,14},{1,9},{3,11},{5,13},{7,15},{16,24},{18,... | collective-permute-start | bytes 786440 | tf_op jit(solution)/shard_map/ppermute | solution.py:19
  16.2 3.5 copy-start.3
  16.2 26.6 %copy-start.2 = (bf16[128,1024]{1,0:T(8,128)(2,1)S(1)}, bf16[128,1024]{1,0:T(8,128)(2,1)}, u32[]{:S(2)}) copy-start(bf16[128,1024]{1,0:T(8,128)(2,1)} %param.16) | copy-start | bytes 786436
  38.8 67.1 %collective-permute-start.1 = (bf16[128,1024]{1,0:T(8,128)(2,1)S(1)}, bf16[128,1024]{1,0:T(8,128)(2,1)S(1)}, u32[]{:S(2)}, u32[]{:S(2)}) collective-permute-start(bf16[128,1024]{1,0:T(8,128)(2,1)S(1)} %copy-done.3), channel_id=1, source_target_pairs={{0,6},{2,8},{4,10},{6,12},{8,14},{1,7},{3,9},{5,11},{7,13},{9,15},... | collective-permute-start | bytes 786440 | tf_op jit(solution)/shard_map/ppermute | solution.py:19
  40.1 65.8 %collective-permute-start.2 = (bf16[128,1024]{1,0:T(8,128)(2,1)S(1)}, bf16[128,1024]{1,0:T(8,128)(2,1)S(1)}, u32[]{:S(2)}, u32[]{:S(2)}) collective-permute-start(bf16[128,1024]{1,0:T(8,128)(2,1)S(1)} %copy-done.3), channel_id=1, source_target_pairs={{0,4},{2,6},{4,8},{6,10},{8,12},{10,14},{1,5},{3,7},{5,9},{7,11},{... | collective-permute-start | bytes 786440 | tf_op jit(solution)/shard_map/ppermute | solution.py:19
  41.4 64.5 %collective-permute-start.3 = (bf16[128,1024]{1,0:T(8,128)(2,1)S(1)}, bf16[128,1024]{1,0:T(8,128)(2,1)S(1)}, u32[]{:S(2)}, u32[]{:S(2)}) collective-permute-start(bf16[128,1024]{1,0:T(8,128)(2,1)S(1)} %copy-done.3), channel_id=1, source_target_pairs={{0,2},{2,4},{4,6},{6,8},{8,10},{10,12},{12,14},{1,3},{3,5},{5,7},{... | collective-permute-start | bytes 786440 | tf_op jit(solution)/shard_map/ppermute | solution.py:19
  106.4 1.0 copy-start.5
  107.0 1.1 copy-start.4
  108.2 1.5 copy-start.7
  126.6 2.6 copy-start.12
  126.6 103.4 %all-gather.12.cloned.1.call-start = ((), (), s32[]{:S(2)}) async-start(), calls=%async_computation.6 | async-start | bytes 4718592 | tf_op jit(solution)/shard_map/all_gather | solution.py:135
  127.3 195.6 %all-gather.8.cloned.1.call-start = ((), (), s32[]{:S(2)}) async-start(), calls=%async_computation.4 | async-start | bytes 4718592 | tf_op jit(solution)/shard_map/all_gather | solution.py:140
  127.9 288.8 %all-gather.10.cloned.1.call-start = ((), (), s32[]{:S(2)}) async-start(), calls=%async_computation.5 | async-start | bytes 4718592 | tf_op jit(solution)/shard_map/all_gather | solution.py:130
  128.5 362.9 %all-gather.14.cloned.1.call-start = ((), (), s32[]{:S(2)}) async-start(), calls=%async_computation.7 | async-start | bytes 4718592 | tf_op jit(solution)/shard_map/all_gather | solution.py:86
  129.1 29.1 %copy-start.6 = (bf16[128,2048]{1,0:T(8,128)(2,1)S(1)}, bf16[128,2048]{1,0:T(8,128)(2,1)}, u32[]{:S(2)}) copy-start(bf16[128,2048]{1,0:T(8,128)(2,1)} %param.14) | copy-start | bytes 1572868
  129.1 29.1 %copy-start.9 = (f32[2048]{0:T(1024)S(1)}, f32[2048]{0:T(1024)}, u32[]{:S(2)}) copy-start(f32[2048]{0:T(1024)} %param.19) | copy-start | bytes 24580
  129.1 375.8 %reduce-scatter.5.cloned.1.call-start = ((), (), s32[]{:S(2)}) async-start(), calls=%async_computation.8 | async-start | bytes 786432 | tf_op jit(solution)/shard_map/reduce_scatter | solution.py:88
  129.8 29.7 %copy-start.10 = (f32[2048]{0:T(1024)S(1)}, f32[2048]{0:T(1024)}, u32[]{:S(2)}) copy-start(f32[2048]{0:T(1024)} %param.21) | copy-start | bytes 24580
  232.9 94.3 %collective-permute-start.12 = (bf16[128,1024]{1,0:T(8,128)(2,1)S(1)}, bf16[128,1024]{1,0:T(8,128)(2,1)S(1)}, u32[]{:S(2)}, u32[]{:S(2)}) collective-permute-start(bf16[128,1024]{1,0:T(8,128)(2,1)S(1)} %convolution_convert_fusion.2), channel_id=1, source_target_pairs={{0,8},{2,10},{4,12},{6,14},{1,9},{3,11},{5,13},{7,15},{16,24},{18,... | collective-permute-start | bytes 786440 | tf_op jit(solution)/shard_map/ppermute | solution.py:19
  234.2 94.3 %collective-permute-start.13 = (bf16[128,1024]{1,0:T(8,128)(2,1)S(1)}, bf16[128,1024]{1,0:T(8,128)(2,1)S(1)}, u32[]{:S(2)}, u32[]{:S(2)}) collective-permute-start(bf16[128,1024]{1,0:T(8,128)(2,1)S(1)} %convolution_convert_fusion.2), channel_id=1, source_target_pairs={{0,6},{2,8},{4,10},{6,12},{8,14},{1,7},{3,9},{5,11},{7,13},{9,15},... | collective-permute-start | bytes 786440 | tf_op jit(solution)/shard_map/ppermute | solution.py:19
  235.5 94.3 %collective-permute-start.14 = (bf16[128,1024]{1,0:T(8,128)(2,1)S(1)}, bf16[128,1024]{1,0:T(8,128)(2,1)S(1)}, u32[]{:S(2)}, u32[]{:S(2)}) collective-permute-start(bf16[128,1024]{1,0:T(8,128)(2,1)S(1)} %convolution_convert_fusion.2), channel_id=1, source_target_pairs={{0,4},{2,6},{4,8},{6,10},{8,12},{10,14},{1,5},{3,7},{5,9},{7,11},{... | collective-permute-start | bytes 786440 | tf_op jit(solution)/shard_map/ppermute | solution.py:19
  236.8 182.9 %collective-permute-start.15 = (bf16[128,1024]{1,0:T(8,128)(2,1)S(1)}, bf16[128,1024]{1,0:T(8,128)(2,1)S(1)}, u32[]{:S(2)}, u32[]{:S(2)}) collective-permute-start(bf16[128,1024]{1,0:T(8,128)(2,1)S(1)} %convolution_convert_fusion.2), channel_id=1, source_target_pairs={{0,2},{2,4},{4,6},{6,8},{8,10},{10,12},{12,14},{1,3},{3,5},{5,7},{... | collective-permute-start | bytes 786440 | tf_op jit(solution)/shard_map/ppermute | solution.py:19
  325.9 94.4 %collective-permute-start.10 = (bf16[128,1024]{1,0:T(8,128)(2,1)S(1)}, bf16[128,1024]{1,0:T(8,128)(2,1)S(1)}, u32[]{:S(2)}, u32[]{:S(2)}) collective-permute-start(bf16[128,1024]{1,0:T(8,128)(2,1)S(1)} %convolution_convert_fusion.4), channel_id=1, source_target_pairs={{0,4},{2,6},{4,8},{6,10},{8,12},{10,14},{1,5},{3,7},{5,9},{7,11},{... | collective-permute-start | bytes 786440 | tf_op jit(solution)/shard_map/ppermute | solution.py:19
  327.2 93.1 %collective-permute-start.11 = (bf16[128,1024]{1,0:T(8,128)(2,1)S(1)}, bf16[128,1024]{1,0:T(8,128)(2,1)S(1)}, u32[]{:S(2)}, u32[]{:S(2)}) collective-permute-start(bf16[128,1024]{1,0:T(8,128)(2,1)S(1)} %convolution_convert_fusion.4), channel_id=1, source_target_pairs={{0,2},{2,4},{4,6},{6,8},{8,10},{10,12},{12,14},{1,3},{3,5},{5,7},{... | collective-permute-start | bytes 786440 | tf_op jit(solution)/shard_map/ppermute | solution.py:19
  328.6 91.8 %collective-permute-start.8 = (bf16[128,1024]{1,0:T(8,128)(2,1)S(1)}, bf16[128,1024]{1,0:T(8,128)(2,1)S(1)}, u32[]{:S(2)}, u32[]{:S(2)}) collective-permute-start(bf16[128,1024]{1,0:T(8,128)(2,1)S(1)} %convolution_convert_fusion.4), channel_id=1, source_target_pairs={{0,8},{2,10},{4,12},{6,14},{1,9},{3,11},{5,13},{7,15},{16,24},{18,... | collective-permute-start | bytes 786440 | tf_op jit(solution)/shard_map/ppermute | solution.py:19
  329.9 90.5 %collective-permute-start.9 = (bf16[128,1024]{1,0:T(8,128)(2,1)S(1)}, bf16[128,1024]{1,0:T(8,128)(2,1)}, u32[]{:S(2)}, u32[]{:S(2)}) collective-permute-start(bf16[128,1024]{1,0:T(8,128)(2,1)S(1)} %convolution_convert_fusion.4), channel_id=1, source_target_pairs={{0,6},{2,8},{4,10},{6,12},{8,14},{1,7},{3,9},{5,11},{7,13},{9,15},... | collective-permute-start | bytes 786440 | tf_op jit(solution)/shard_map/ppermute | solution.py:19
  424.3 1.5 copy-start.8
  491.4 14.6 %copy-start.11 = (f32[2048]{0:T(1024)S(1)}, f32[2048]{0:T(1024)}, u32[]{:S(2)}) copy-start(f32[2048]{0:T(1024)} %param.26) | copy-start | bytes 24580
  491.4 18.7 %copy-start.1 = (f32[8,257]{1,0:T(8,128)S(1)}, f32[8,257]{1,0:T(8,128)}, u32[]{:S(2)}) copy-start(f32[8,257]{1,0:T(8,128)} %param.18) | copy-start | bytes 24676
Sparse Core Ops, SparseCore 0:
  9.4 113.4 all-gather.5
  126.7 30.2 reduce-scatter.2
  159.2 70.7 all-gather.11
  232.0 90.9 all-gather.7
  325.0 91.6 all-gather.9
  418.6 72.8 all-gather.13
  495.3 9.5 reduce-scatter.4
where the time goes:
time: 519 us; the launch traced here: 517 us
  waiting for transfers between devices  416 us (80%)
  matrix products  37.2 us (7%)
  starting transfers between devices  20.9 us (4%)
  local copies, waits for them, and re-layouts  18.1 us (3%)
  between operations  14.6 us (3%)
  other arithmetic  6.07 us (1%)
    all_gather x1, waiting for transfers between devices, shards(): lax.all_gather(query_weight, 'sp', axis=0, tiled=True)  85.5 us
    all_gather x1, waiting for transfers between devices, shards(): lax.all_gather(value_weight, 'sp', axis=0, tiled=True)  84.8 us
    ppermute x16, waiting for transfers between devices, from_behind(): lax.ppermute(value, axis, [(source, source + steps) for source in range(i...  80.9 us
    all_gather x1, waiting for transfers between devices, shards(): lax.all_gather(key_weight, 'sp', axis=0, tiled=True)  68 us
    all_gather x2, waiting for transfers between devices, combine(): lax.all_gather(weight, 'sp', axis=1, tiled=True)  58.8 us
    reduce_scatter x2, waiting for transfers between devices, combine(): lax.psum_scatter(partial_rows.astype(jnp.bfloat16), 'tp', scatter_dimensi...  34.5 us
    ppermute x16, starting transfers between devices, from_behind(): lax.ppermute(value, axis, [(source, source + steps) for source in range(i...  20.7 us
    unnamed x97, local copies, waits for them, and re-layouts  12.4 us
  transfers between devices with their start and end apart: 23, of which 9 were waited for; matrix products, arithmetic and copies ran while one was open for 9% of the time, Pallas kernels for 0%

commit v1 on v0

--- a/solution.py
+++ b/solution.py
@@ -1,7 +1,13 @@
 import jax
 import jax.numpy as jnp
 from jax import lax
+from jax.experimental import pallas as pl
+from jax.experimental.pallas import tpu as pltpu
 from jax.sharding import PartitionSpec as P
+
+MESH = pl.DeviceIdType.MESH
+BF16 = jnp.bfloat16
+F32 = jnp.float32
 
 SEG = 64
 LEFT = 8
@@ -112,6 +118,18 @@
     out_second,
 ):
     tok_rows = resid.shape[0]
+    n_sp = lax.axis_size("sp")
+    if (
+        rel_first.shape[0] == n_sp
+        and n_sp % 2 == 0
+        and lax.axis_size("tp") == 2
+        and REACH % tok_rows == 0
+        and tok_rows == REL_CLIP
+    ):
+        return by_heads(
+            resid, queries_first, keys_first, values_first, rel_first, post_first, out_first,
+            pre_second, query_weight, key_weight, value_weight, rel_second, post_second, out_second,
+        )
     depth = (REACH + tok_rows - 1) // tok_rows
     anchor = lax.axis_index("sp") * tok_rows
     key_live = anchor - REACH + jnp.arange(tok_rows + REACH, dtype=jnp.int32) >= 0
@@ -153,6 +171,362 @@
     return full_rows(hidden_two)
 
 
+def scaled(values):
+    return values * lax.rsqrt(jnp.mean(values * values, axis=-1, keepdims=True) + EPS)
+
+
+def build_kernel(n, tok, head, width, reach):
+    share = tok // 2
+    cols = width // n
+    span = reach + tok
+    model = width
+
+    def kernel(
+        q_hbm, k_hbm, v_hbm, wq_hbm, wk_hbm, wv_hbm, resid_hbm, o1_hbm, o2_hbm,
+        rel1, rel2, post1, pre2, post2,
+        out_ref,
+        heads, weights, outs, res, bias, mixed1, mixed2, parts1, parts2, branch1, branch2, rows2, last,
+        loc_sem, hs, hr, ws, wr, fs, fr, gs, gr, bs, br, xs, xr, ys, yr,
+    ):
+        s = lax.axis_index("sp")
+        t = lax.axis_index("tp")
+        u = 1 - t
+        side = s + 1 - 2 * lax.rem(s, 2)
+
+        def rcopy(src, dst, ssem, rsem, sp, tp):
+            return pltpu.make_async_remote_copy(
+                src_ref=src, dst_ref=dst, send_sem=ssem, recv_sem=rsem,
+                device_id={"sp": sp, "tp": tp}, device_id_type=MESH,
+            )
+
+        def peer(k):
+            return lax.rem(s + k, n)
+
+        barrier = pltpu.get_barrier_semaphore()
+        for k in range(n):
+            if k:
+                pl.semaphore_signal(
+                    barrier, inc=1, device_id={"sp": peer(k), "tp": t}, device_id_type=MESH
+                )
+            pl.semaphore_signal(
+                barrier, inc=1, device_id={"sp": peer(k), "tp": u}, device_id_type=MESH
+            )
+        pl.semaphore_wait(barrier, 2 * n - 1)
+
+        def lanes(j):
+            return pl.ds(pl.multiple_of(j * head, head), head)
+
+        def trows(j, base=0):
+            return pl.ds(pl.multiple_of(base + j * tok, tok), tok)
+
+        wrows = width // n
+
+        def head_copy(i, ref, j, src):
+            dst = heads.at[i, trows(src, reach)]
+            return rcopy(ref.at[:, lanes(j)], dst, hs.at[i, j], hr.at[i, src], j, t)
+
+        def weight_copy(i, ref, j, src):
+            dst = weights.at[
+                pl.ds(pl.multiple_of(src * wrows, wrows), wrows), pl.ds(i * head, head)
+            ]
+            return rcopy(ref.at[:, lanes(j)], dst, ws.at[i, j], wr.at[i, src], j, t)
+
+        qkv = (q_hbm, k_hbm, v_hbm)
+        wqkv = (wq_hbm, wk_hbm, wv_hbm)
+        for k in range(1, n):
+            for i in range(3):
+                head_copy(i, qkv[i], peer(k), s).start()
+        for i in range(3):
+            pltpu.make_async_copy(
+                qkv[i].at[:, lanes(s)], heads.at[i, trows(s, reach)], hr.at[i, s]
+            ).start()
+        for k in range(1, n):
+            for i in range(3):
+                weight_copy(i, wqkv[i], peer(k), s).start()
+        for i in range(3):
+            pltpu.make_async_copy(
+                wqkv[i].at[:, lanes(s)],
+                weights.at[pl.ds(pl.multiple_of(s * wrows, wrows), wrows), pl.ds(i * head, head)],
+                wr.at[i, s],
+            ).start()
+        local = [
+            pltpu.make_async_copy(o1_hbm, outs.at[0], loc_sem.at[0]),
+            pltpu.make_async_copy(o2_hbm, outs.at[1], loc_sem.at[1]),
+            pltpu.make_async_copy(
+                resid_hbm.at[pl.ds(pl.multiple_of(t * share, share), share)], res, loc_sem.at[2]
+            ),
+        ]
+        for copy in local:
+            copy.start()
+
+        near = 2 * REL_CLIP
+        query = lax.broadcasted_iota(jnp.int32, (tok, span), 0) // SEG
+        key = lax.broadcasted_iota(jnp.int32, (tok, span), 1) // SEG
+        live = (key >= query) & (key <= query + LEFT)
+        for layer, rel in enumerate((rel1, rel2)):
+            line = rel[pl.ds(s, 1), :]
+            spread = jnp.broadcast_to(line, (tok, line.shape[1]))
+            row = lax.broadcasted_iota(jnp.int32, spread.shape, 0)
+            step = 1
+            while step < tok:
+                moved = pltpu.roll(spread, step, 1)
+                spread = jnp.where(lax.rem(row // step, 2) == 1, moved, spread)
+                step *= 2
+            far = jnp.broadcast_to(line[:, near : near + 1], (tok, span - near))
+            whole = jnp.concatenate([far, spread[:, :near]], axis=1)
+            bias[layer] = jnp.where(live, whole, NEG_FILL)
+
+        heads[1, :reach] = jnp.zeros((reach, head), BF16)
+        heads[2, :reach] = jnp.zeros((reach, head), BF16)
+
+        def attend(layer, b):
+            q = heads[0, trows(b, reach)]
+            k = heads[1, pl.ds(pl.multiple_of(b * tok, tok), span)]
+            v = heads[2, pl.ds(pl.multiple_of(b * tok, tok), span)]
+            scores = lax.dot_general(
+                q, k, (((1,), (1,)), ((), ())), preferred_element_type=F32
+            ) * head ** (-0.5) + bias[layer]
+            column = lax.broadcasted_iota(jnp.int32, scores.shape, 1)
+            scores = jnp.where(column >= reach - b * tok, scores, NEG_FILL)
+            e = jnp.exp(scores - jnp.max(scores, axis=-1, keepdims=True))
+            e = (e * (1.0 / jnp.sum(e, axis=-1, keepdims=True))).astype(BF16)
+            return jnp.dot(e, v, preferred_element_type=F32).astype(BF16)
+
+        def layer_branch(layer, mixed, parts, branch, ms, mr, ps, pr, wait_block):
+            def mcopy(b, src, k, sp):
+                block = mixed.at[src, trows(b)]
+                return rcopy(block, block, ms.at[b, k], mr.at[b, src], sp, t)
+
+            half = n // 2
+
+            def own(b, _):
+                wait_block(b)
+                mixed[s, trows(b)] = attend(layer, b)
+                mcopy(b, s, 0, side).start()
+                for k in range(1, half):
+                    mcopy(b, s, k, peer(2 * k)).start()
+                return 0
+
+            lax.fori_loop(0, n, own, 0)
+
+            def pcopy(b, c):
+                return rcopy(
+                    parts.at[b, c], branch.at[t, s], ps.at[b, c], pr.at[t, s], b, c
+                )
+
+            def forward(b):
+                for k in range(1, half):
+                    mcopy(b, peer(2 * k), k, side).wait_recv()
+                    mcopy(b, peer(2 * k), half - 1 + k, side).start()
+
+            def project(b):
+                for k in range(half):
+                    mcopy(b, lax.rem(side + 2 * k, n), k, side).wait_recv()
+                lhs = jnp.concatenate([mixed[j, trows(b)] for j in range(n)], axis=1)
+                part = jnp.dot(lhs, outs[layer], preferred_element_type=F32).astype(BF16)
+                parts[b, 0] = part[:share]
+                parts[b, 1] = part[share:]
+                pcopy(b, u).start()
+
+                @pl.when(b != s)
+                def _():
+                    pcopy(b, t).start()
+
+                @pl.when(b == s)
+                def _():
+                    pltpu.make_async_copy(
+                        parts.at[b, t], branch.at[t, s], pr.at[t, s]
+                    ).start()
+
+            def step(b, _):
+                forward(b)
+
+                @pl.when(b > 0)
+                def _():
+                    project(b - 1)
+
+                return 0
+
+            lax.fori_loop(0, n, step, 0)
+            project(n - 1)
+
+            def arrived(j, _):
+                for c in range(2):
+                    rcopy(
+                        parts.at[0, 0], branch.at[c, j], ps.at[0, 0], pr.at[c, j], side, t
+                    ).wait_recv()
+                return 0
+
+            lax.fori_loop(0, n, arrived, 0)
+
+            def drain(b, _):
+                for k in range(2 * half - 1):
+                    mcopy(b, s, k, side).wait_send()
+                pcopy(b, u).wait_send()
+
+                @pl.when(b != s)
+                def _():
+                    pcopy(b, t).wait_send()
+
+                return 0
+
+            total = [
+                jnp.concatenate([branch[c, j] for j in range(n)], axis=1).astype(F32)
+                for c in range(2)
+            ]
+            return (total[0] + total[1]).astype(BF16).astype(F32), drain
+
+        def heads_ready(b):
+            for i in range(3):
+                head_copy(i, qkv[i], side, b).wait_recv()
+
+        local[0].wait()
+        local[1].wait()
+        values, drain1 = layer_branch(
+            0, mixed1, parts1, branch1, fs, fr, bs.at[0], br.at[0], heads_ready
+        )
+        local[2].wait()
+        hidden = (res[...].astype(F32) + scaled(values) * post1[...]).astype(BF16)
+        res[...] = hidden
+        rows2[2 * s + t] = (scaled(hidden.astype(F32)) * pre2[...]).astype(BF16)
+
+        def xcopy(src, c, k, sp, tp):
+            block = rows2.at[2 * src + c]
+            return rcopy(block, block, xs.at[src, k], xr.at[2 * src + c], sp, tp)
+
+        half = n // 2
+        xcopy(s, t, 0, side, t).start()
+        for k in range(1, half):
+            xcopy(s, t, k + 1, peer(2 * k), t).start()
+        xcopy(s, t, 1, s, u).start()
+        for k in range(1, half):
+            src = peer(2 * k)
+            xcopy(src, t, 0, side, t).wait_recv()
+            xcopy(src, t, 0, side, t).start()
+            xcopy(src, t, 1, s, u).start()
+
+        def weights_ready(j, _):
+            for i in range(3):
+                weight_copy(i, wqkv[i], side, j).wait_recv()
+            return 0
+
+        lax.fori_loop(0, n, weights_ready, 0)
+
+        def project_rows(src):
+            xcopy(src, u, 1, s, u).wait_recv()
+            lhs = rows2[pl.ds(2 * src, 2)].reshape(tok, model)
+            got = jnp.dot(lhs, weights[...], preferred_element_type=F32).astype(BF16)
+            for i in range(3):
+                heads[i, trows(src, reach)] = got[:, i * head : (i + 1) * head]
+
+        def near_rows(k, _):
+            src = lax.rem(side + 2 * k, n)
+            xcopy(src, t, 0, side, t).wait_recv()
+            xcopy(src, t, 1, s, u).start()
+            project_rows(lax.rem(s + 2 * k, n))
+            return 0
+
+        lax.fori_loop(0, half, near_rows, 0)
+
+        def far_rows(k, _):
+            project_rows(lax.rem(side + 2 * k, n))
+            return 0
+
+        lax.fori_loop(0, half, far_rows, 0)
+
+        values, drain2 = layer_branch(
+            1, mixed2, parts2, branch2, gs, gr, bs.at[1], br.at[1], lambda b: None
+        )
+        done = (res[...].astype(F32) + scaled(values) * post2[...]).astype(BF16)
+        last[t] = done
+        final = rcopy(last.at[t], last.at[t], ys, yr, s, u)
+        final.start()
+
+        lax.fori_loop(0, n, lambda b, c: drain1(b, c), 0)
+        lax.fori_loop(0, n, lambda b, c: drain2(b, c), 0)
+        for k in range(1, n):
+            for i in range(3):
+                head_copy(i, qkv[i], peer(k), s).wait_send()
+                weight_copy(i, wqkv[i], peer(k), s).wait_send()
+        for k in range(half + 1):
+            xcopy(s, t, k, side, t).wait_send()
+        for k in range(1, half):
+            xcopy(peer(2 * k), t, 0, side, t).wait_send()
+            xcopy(peer(2 * k), t, 1, side, t).wait_send()
+        for k in range(half):
+            xcopy(lax.rem(side + 2 * k, n), t, 1, side, t).wait_send()
+        final.wait_send()
+        rcopy(last.at[u], last.at[u], ys, yr, s, u).wait_recv()
+        out_ref[:share] = last[0]
+        out_ref[share:] = last[1]
+
+    half = n // 2
+    scratch = [
+        pltpu.VMEM((3, reach + n * tok, head), BF16),
+        pltpu.VMEM((width, 3 * head), BF16),
+        pltpu.VMEM((2, n * head, cols), BF16),
+        pltpu.VMEM((share, width), BF16),
+        pltpu.VMEM((2, tok, span), F32),
+        pltpu.VMEM((n, n * tok, head), BF16),
+        pltpu.VMEM((n, n * tok, head), BF16),
+        pltpu.VMEM((n, 2, share, cols), BF16),
+        pltpu.VMEM((n, 2, share, cols), BF16),
+        pltpu.VMEM((2, n, share, cols), BF16),
+        pltpu.VMEM((2, n, share, cols), BF16),
+        pltpu.VMEM((2 * n, share, width), BF16),
+        pltpu.VMEM((2, share, width), BF16),
+        pltpu.SemaphoreType.DMA((3,)),
+        pltpu.SemaphoreType.DMA((3, n)),
+        pltpu.SemaphoreType.DMA((3, n)),
+        pltpu.SemaphoreType.DMA((3, n)),
+        pltpu.SemaphoreType.DMA((3, n)),
+        pltpu.SemaphoreType.DMA((n, 2 * half - 1)),
+        pltpu.SemaphoreType.DMA((n, n)),
+        pltpu.SemaphoreType.DMA((n, 2 * half - 1)),
+        pltpu.SemaphoreType.DMA((n, n)),
+        pltpu.SemaphoreType.DMA((2, n, 2)),
+        pltpu.SemaphoreType.DMA((2, 2, n)),
+        pltpu.SemaphoreType.DMA((n, half + 1)),
+        pltpu.SemaphoreType.DMA((2 * n,)),
+        pltpu.SemaphoreType.DMA,
+        pltpu.SemaphoreType.DMA,
+    ]
+    return kernel, scratch
+
+
+def reversed_line(table, tok):
+    top = table[:, -1:]
+    return jnp.concatenate(
+        [table[:, :0:-1], jnp.broadcast_to(top, (table.shape[0], tok))], axis=1
+    )
+
+
+def by_heads(
+    resid, queries_first, keys_first, values_first, rel_first, post_first, out_first, pre_second,
+    query_weight, key_weight, value_weight, rel_second, post_second, out_second,
+):
+    n = lax.axis_size("sp")
+    tok, width = resid.shape
+    head = queries_first.shape[1] // rel_first.shape[0]
+    kernel, scratch = build_kernel(n, tok, head, width, REACH)
+    hbm = pl.BlockSpec(memory_space=pl.ANY)
+    vmem = pl.BlockSpec(memory_space=pltpu.VMEM)
+    return pl.pallas_call(
+        kernel,
+        out_shape=jax.ShapeDtypeStruct((tok, width), BF16),
+        in_specs=[hbm] * 9 + [vmem] * 5,
+        out_specs=vmem,
+        scratch_shapes=scratch,
+        compiler_params=pltpu.CompilerParams(
+            collective_id=0, has_side_effects=True, vmem_limit_bytes=40 * 2**20
+        ),
+    )(
+        queries_first, keys_first, values_first, query_weight, key_weight, value_weight, resid,
+        out_first, out_second, reversed_line(rel_first, tok), reversed_line(rel_second, tok),
+        post_first[None], pre_second[None], post_second[None],
+    )
+
+
 def solution(mesh):
     in_specs = (
         P(("grp", "sp"), None),

time: 519 us -> 201 us (0.39)
  waiting for transfers between devices: 416 us -> 0 us
  Pallas kernels: 0 us -> 187 us
  matrix products: 37.2 us -> 0 us
  starting transfers between devices: 20.9 us -> 0 us
  between operations: 14.6 us -> 0.03 us
  other arithmetic: 6.07 us -> 0.01 us
    all_gather x5 -> x0, waiting for transfers between devices: 297 us -> none  [the longest x1 85.5 us: shards(): lax.all_gather(query_weight, 'sp', axis=0, tiled=True)]
    pallas_call x0 -> x1, Pallas kernels: none -> 187 us  [by_heads(): pl.pallas_call(kernel, out_shape=jax.ShapeDtypeStruct((tok, width), BF16)...]
    ppermute x16 -> x0, waiting for transfers between devices: 80.9 us -> none  [from_behind(): lax.ppermute(value, axis, [(source, source + steps) for source in range(i...]
    reduce_scatter x2 -> x0, waiting for transfers between devices: 34.5 us -> none  [combine(): lax.psum_scatter(partial_rows.astype(jnp.bfloat16), 'tp', scatter_dimensi...]
    dot_general x11 -> x0, matrix products: 32.2 us -> none  [the longest x2 9.76 us: attend_band(): jnp.einsum('nhqk,nkhd->nqhd', weights, value_band, preferred_element_type...]
    ppermute x16 -> x0, starting transfers between devices: 20.7 us -> none  [from_behind(): lax.ppermute(value, axis, [(source, source + steps) for source in range(i...]
    unnamed x97 -> x29, local copies, waits for them, and re-layouts: 12.4 us -> 11.1 us
  transfers between devices with their start and end apart: 23 -> 0, of which waited for: 9 -> 0; matrix products, arithmetic and copies ran while one was open for 9% -> 0% of each run, Pallas kernels for 0% -> 0%
where the time goes in v1:
time: 201 us; the launch traced here: 200 us
  Pallas kernels  187 us (93%)
  local copies, waits for them, and re-layouts  13.4 us (7%)
    pallas_call x1, Pallas kernels, by_heads(): pl.pallas_call(kernel, out_shape=jax.ShapeDtypeStruct((tok, width), BF16)...  187 us
    unnamed x29, local copies, waits for them, and re-layouts  11.1 us

profile of v1, /device:TPU:29, one launch (start us, length us, event | category | flops | bytes accessed | tf_op | source)
XLA Modules:
  0.0 200.0 jit_solution(797899726214722288)
XLA Ops:
  0.0 0.0 copy-start.12
  0.0 0.9 slice_reduce_fusion.1
  0.9 0.8 slice_reduce_fusion
  1.7 0.1 broadcast_in_dim.26
  1.8 0.1 broadcast_in_dim.24
  1.8 0.0 copy-done.12
  1.8 0.0 copy-start.13
  1.8 0.1 slice.12
  1.9 0.1 rev.6
  2.0 0.5 copy-done.13
  2.5 0.1 slice.14
  2.6 0.1 rev.7
  2.8 0.0 copy-start.9
  2.8 0.0 copy-start.10
  2.8 0.0 copy-start.11
  2.8 0.7 copy-done.9
  3.5 0.0 copy-done.10
  3.5 0.0 copy-done.11
  3.5 0.0 copy-start
  3.5 1.0 copy-done
  4.5 0.0 copy-start.1
  4.5 1.0 copy-done.1
  5.6 0.0 copy-start.2
  5.6 1.0 copy-done.2
  6.6 0.0 copy-start.3
  6.6 1.0 copy-done.3
  7.7 0.0 copy-start.4
  7.7 1.0 copy-done.4
  8.7 0.0 copy-start.5
  8.7 1.0 copy-done.5
  9.7 0.0 copy-start.6
  9.7 0.9 copy-done.6
  10.7 0.0 copy-start.7
  10.7 0.9 copy-done.7
  11.6 0.0 copy-start.8
  11.6 0.9 copy-done.8
  12.6 186.6 %shard_map.136 = bf16[128,2048]{1,0:T(8,128)(2,1)S(1)} custom-call(bf16[128,1024]{1,0:T(8,128)(2,1)S(1)} %copy-done.6, bf16[128,1024]{1,0:T(8,128)(2,1)S(1)} %copy-done.7, bf16[128,1024]{1,0:T(8,128)(2,1)S(1)} %copy-done.8, bf16[256,1024]{1,0:T(8,128)(2,1)S(1)} %copy-done, bf16[256,1024]{1,0:T(8,128)(2,1)S(1)} %copy-done.1, bf16[256,1024]{1,0:T(8,128)(2,1)S(1)} %copy-done.2, ...), custom_call_target="tpu_custom_call" | custom-call | tf_op jit(solution)/shard_map/pallas_call | solution.py:514
  199.2 0.8 copy.16
  (1 shorter events, 0.0 us)
Async XLA Ops:
  0.0 1.8 copy-start.12
  1.8 0.7 copy-start.13
  2.8 0.7 copy-start.9
  2.8 0.7 copy-start.10
  2.8 0.7 copy-start.11
  3.5 1.0 copy-start
  4.5 1.0 copy-start.1
  5.6 1.0 copy-start.2
  6.6 1.0 copy-start.3
  7.7 1.0 copy-start.4
  8.7 1.0 copy-start.5
  9.7 0.9 copy-start.6
  10.7 0.9 copy-start.7
  11.6 0.9 copy-start.8

commit v2 on v1

--- a/solution.py
+++ b/solution.py
@@ -123,6 +123,7 @@
         rel_first.shape[0] == n_sp
         and n_sp % 2 == 0
         and lax.axis_size("tp") == 2
+        and lax.axis_size("grp") == 2
         and REACH % tok_rows == 0
         and tok_rows == REL_CLIP
     ):
@@ -185,18 +186,19 @@
         q_hbm, k_hbm, v_hbm, wq_hbm, wk_hbm, wv_hbm, resid_hbm, o1_hbm, o2_hbm,
         rel1, rel2, post1, pre2, post2,
         out_ref,
-        heads, weights, outs, res, bias, mixed1, mixed2, parts1, parts2, branch1, branch2, rows2, last,
-        loc_sem, hs, hr, ws, wr, fs, fr, gs, gr, bs, br, xs, xr, ys, yr,
+        heads, weights, outs, res, bias, mixed1, mixed2, parts, inbox, joined, branch, rows2, last,
+        loc_sem, hs, hr, ws, wr, wf, fs, fr, gs, gr, ps, pr, bs, br, xs, xr, ys, yr,
     ):
         s = lax.axis_index("sp")
         t = lax.axis_index("tp")
+        g = lax.axis_index("grp")
         u = 1 - t
         side = s + 1 - 2 * lax.rem(s, 2)
 
-        def rcopy(src, dst, ssem, rsem, sp, tp):
+        def rcopy(src, dst, ssem, rsem, sp, tp, grp=g):
             return pltpu.make_async_remote_copy(
                 src_ref=src, dst_ref=dst, send_sem=ssem, recv_sem=rsem,
-                device_id={"sp": sp, "tp": tp}, device_id_type=MESH,
+                device_id={"grp": grp, "sp": sp, "tp": tp}, device_id_type=MESH,
             )
 
         def peer(k):
@@ -211,7 +213,10 @@
             pl.semaphore_signal(
                 barrier, inc=1, device_id={"sp": peer(k), "tp": u}, device_id_type=MESH
             )
-        pl.semaphore_wait(barrier, 2 * n - 1)
+        pl.semaphore_signal(
+            barrier, inc=1, device_id={"grp": 1 - g, "sp": s, "tp": t}, device_id_type=MESH
+        )
+        pl.semaphore_wait(barrier, 2 * n)
 
         def lanes(j):
             return pl.ds(pl.multiple_of(j * head, head), head)
@@ -225,11 +230,30 @@
             dst = heads.at[i, trows(src, reach)]
             return rcopy(ref.at[:, lanes(j)], dst, hs.at[i, j], hr.at[i, src], j, t)
 
-        def weight_copy(i, ref, j, src):
-            dst = weights.at[
-                pl.ds(pl.multiple_of(src * wrows, wrows), wrows), pl.ds(i * head, head)
-            ]
-            return rcopy(ref.at[:, lanes(j)], dst, ws.at[i, j], wr.at[i, src], j, t)
+        hrows = wrows // 2
+
+        def weight_half(i, src, part):
+            start = pl.multiple_of(src * wrows + part * hrows, hrows)
+            return weights.at[pl.ds(start, hrows), pl.ds(i * head, head)]
+
+        def weight_copy(i, j, src):
+            piece = wqkv[i].at[pl.ds(pl.multiple_of(g * hrows, hrows), hrows), lanes(j)]
+            return rcopy(piece, weight_half(i, src, g), ws.at[i, j], wr.at[i, src, g], j, t)
+
+        def weight_hand(i, src):
+            piece = weight_half(i, src, g)
+            return rcopy(piece, piece, wf.at[i, src], wr.at[i, src, g], s, t, 1 - g)
+
+        def weight_handed(i, src):
+            piece = weight_half(i, src, 1 - g)
+            return rcopy(piece, piece, wf.at[i, src], wr.at[i, src, 1 - g], s, t, 1 - g)
+
+        def own_weights(i):
+            return pltpu.make_async_copy(
+                wqkv[i].at[:, lanes(s)],
+                weights.at[pl.ds(pl.multiple_of(s * wrows, wrows), wrows), pl.ds(i * head, head)],
+                wr.at[i, s, 0],
+            )
 
         qkv = (q_hbm, k_hbm, v_hbm)
         wqkv = (wq_hbm, wk_hbm, wv_hbm)
@@ -240,15 +264,14 @@
             pltpu.make_async_copy(
                 qkv[i].at[:, lanes(s)], heads.at[i, trows(s, reach)], hr.at[i, s]
             ).start()
-        for k in range(1, n):
+        for i in range(3):
+            own_weights(i).start()
+
+        def send_weights():
             for i in range(3):
-                weight_copy(i, wqkv[i], peer(k), s).start()
-        for i in range(3):
-            pltpu.make_async_copy(
-                wqkv[i].at[:, lanes(s)],
-                weights.at[pl.ds(pl.multiple_of(s * wrows, wrows), wrows), pl.ds(i * head, head)],
-                wr.at[i, s],
-            ).start()
+                for k in range(1, n):
+                    weight_copy(i, peer(k), s).start()
+
         local = [
             pltpu.make_async_copy(o1_hbm, outs.at[0], loc_sem.at[0]),
             pltpu.make_async_copy(o2_hbm, outs.at[1], loc_sem.at[1]),
@@ -264,15 +287,25 @@
         key = lax.broadcasted_iota(jnp.int32, (tok, span), 1) // SEG
         live = (key >= query) & (key <= query + LEFT)
         for layer, rel in enumerate((rel1, rel2)):
-            line = rel[pl.ds(s, 1), :]
-            spread = jnp.broadcast_to(line, (tok, line.shape[1]))
+            table = rel[pl.ds(s, 1), :]
+            top = table[:, near : near + 1]
+            entry = lax.broadcasted_iota(jnp.int32, (near, near + tok), 0)
+            place = lax.broadcasted_iota(jnp.int32, (near, near + tok), 1)
+            flip = (entry + place == near).astype(F32)
+            line = jnp.dot(
+                jnp.broadcast_to(table[:, :near], (8, near)), flip,
+                preferred_element_type=F32, precision=lax.Precision.HIGHEST,
+            )[:1]
+            spot = lax.broadcasted_iota(jnp.int32, line.shape, 1)
+            line = jnp.where((spot == 0) | (spot >= near), top, line)
+            spread = jnp.broadcast_to(line, (tok, near + tok))
             row = lax.broadcasted_iota(jnp.int32, spread.shape, 0)
             step = 1
             while step < tok:
                 moved = pltpu.roll(spread, step, 1)
                 spread = jnp.where(lax.rem(row // step, 2) == 1, moved, spread)
                 step *= 2
-            far = jnp.broadcast_to(line[:, near : near + 1], (tok, span - near))
+            far = jnp.broadcast_to(top, (tok, span - near))
             whole = jnp.concatenate([far, spread[:, :near]], axis=1)
             bias[layer] = jnp.where(live, whole, NEG_FILL)
 
@@ -292,7 +325,7 @@
             e = (e * (1.0 / jnp.sum(e, axis=-1, keepdims=True))).astype(BF16)
             return jnp.dot(e, v, preferred_element_type=F32).astype(BF16)
 
-        def layer_branch(layer, mixed, parts, branch, ms, mr, ps, pr, wait_block):
+        def layer_branch(layer, mixed, ms, mr, wait_block, after_own):
             def mcopy(b, src, k, sp):
                 block = mixed.at[src, trows(b)]
                 return rcopy(block, block, ms.at[b, k], mr.at[b, src], sp, t)
@@ -308,10 +341,18 @@
                 return 0
 
             lax.fori_loop(0, n, own, 0)
-
-            def pcopy(b, c):
+            after_own()
+
+            def pcopy(b):
                 return rcopy(
-                    parts.at[b, c], branch.at[t, s], ps.at[b, c], pr.at[t, s], b, c
+                    parts.at[layer, b, u], inbox.at[layer, b],
+                    ps.at[layer, b], pr.at[layer, b], s, u,
+                )
+
+            def bcopy(b, src):
+                return rcopy(
+                    joined.at[layer, b], branch.at[layer, src],
+                    bs.at[layer, b], br.at[layer, src], b, t,
                 )
 
             def forward(b):
@@ -324,18 +365,23 @@
                     mcopy(b, lax.rem(side + 2 * k, n), k, side).wait_recv()
                 lhs = jnp.concatenate([mixed[j, trows(b)] for j in range(n)], axis=1)
                 part = jnp.dot(lhs, outs[layer], preferred_element_type=F32).astype(BF16)
-                parts[b, 0] = part[:share]
-                parts[b, 1] = part[share:]
-                pcopy(b, u).start()
+                parts[layer, b, 0] = part[:share]
+                parts[layer, b, 1] = part[share:]
+                pcopy(b).start()
+
+            def join(b):
+                pcopy(b).wait_recv()
+                total = parts[layer, b, t].astype(F32) + inbox[layer, b].astype(F32)
+                joined[layer, b] = total.astype(BF16)
 
                 @pl.when(b != s)
                 def _():
-                    pcopy(b, t).start()
+                    bcopy(b, s).start()
 
                 @pl.when(b == s)
                 def _():
                     pltpu.make_async_copy(
-                        parts.at[b, t], branch.at[t, s], pr.at[t, s]
+                        joined.at[layer, b], branch.at[layer, s], br.at[layer, s]
                     ).start()
 
             def step(b, _):
@@ -345,16 +391,19 @@
                 def _():
                     project(b - 1)
 
+                @pl.when(b > 1)
+                def _():
+                    join(b - 2)
+
                 return 0
 
             lax.fori_loop(0, n, step, 0)
             project(n - 1)
+            join(n - 2)
+            join(n - 1)
 
             def arrived(j, _):
-                for c in range(2):
-                    rcopy(
-                        parts.at[0, 0], branch.at[c, j], ps.at[0, 0], pr.at[c, j], side, t
-                    ).wait_recv()
+                bcopy(side, j).wait_recv()
                 return 0
 
             lax.fori_loop(0, n, arrived, 0)
@@ -362,19 +411,16 @@
             def drain(b, _):
                 for k in range(2 * half - 1):
                     mcopy(b, s, k, side).wait_send()
-                pcopy(b, u).wait_send()
+                pcopy(b).wait_send()
 
                 @pl.when(b != s)
                 def _():
-                    pcopy(b, t).wait_send()
+                    bcopy(b, s).wait_send()
 
                 return 0
 
-            total = [
-                jnp.concatenate([branch[c, j] for j in range(n)], axis=1).astype(F32)
-                for c in range(2)
-            ]
-            return (total[0] + total[1]).astype(BF16).astype(F32), drain
+            values = jnp.concatenate([branch[layer, j] for j in range(n)], axis=1)
+            return values.astype(F32), drain
 
         def heads_ready(b):
             for i in range(3):
@@ -382,61 +428,80 @@
 
         local[0].wait()
         local[1].wait()
-        values, drain1 = layer_branch(
-            0, mixed1, parts1, branch1, fs, fr, bs.at[0], br.at[0], heads_ready
-        )
+        values, drain1 = layer_branch(0, mixed1, fs, fr, heads_ready, send_weights)
         local[2].wait()
         hidden = (res[...].astype(F32) + scaled(values) * post1[...]).astype(BF16)
         res[...] = hidden
         rows2[2 * s + t] = (scaled(hidden.astype(F32)) * pre2[...]).astype(BF16)
 
-        def xcopy(src, c, k, sp, tp):
-            block = rows2.at[2 * src + c]
-            return rcopy(block, block, xs.at[src, k], xr.at[2 * src + c], sp, tp)
-
         half = n // 2
-        xcopy(s, t, 0, side, t).start()
-        for k in range(1, half):
-            xcopy(s, t, k + 1, peer(2 * k), t).start()
-        xcopy(s, t, 1, s, u).start()
-        for k in range(1, half):
-            src = peer(2 * k)
-            xcopy(src, t, 0, side, t).wait_recv()
-            xcopy(src, t, 0, side, t).start()
-            xcopy(src, t, 1, s, u).start()
-
-        def weights_ready(j, _):
+        wide = width // half
+
+        def xcopy(src, c, k, sp, tp, m):
+            block = rows2.at[2 * src + c, :, pl.ds(pl.multiple_of(m * wide, wide), wide)]
+            return rcopy(block, block, xs.at[src, k, m], xr.at[2 * src + c, m], sp, tp)
+
+        def xsend(m, _):
+            for k in range(1, half):
+                xcopy(s, t, k + 1, peer(2 * k), t, m).start()
+            xcopy(s, t, 0, side, t, m).start()
+            xcopy(s, t, 1, s, u, m).start()
+            return 0
+
+        lax.fori_loop(0, half, xsend, 0)
+
+        def hand_weights(k, _):
             for i in range(3):
-                weight_copy(i, wqkv[i], side, j).wait_recv()
-            return 0
-
-        lax.fori_loop(0, n, weights_ready, 0)
+                weight_copy(i, side, peer(k)).wait_recv()
+                weight_hand(i, peer(k)).start()
+            return 0
+
+        lax.fori_loop(1, n, hand_weights, 0)
+
+        def near_rows(m, _):
+            for k in range(1, half):
+                src = peer(2 * k)
+                xcopy(src, t, 0, side, t, m).wait_recv()
+                xcopy(src, t, 0, side, t, m).start()
+                xcopy(src, t, 1, s, u, m).start()
+            return 0
+
+        lax.fori_loop(0, half, near_rows, 0)
+
+        def weights_ready(k, _):
+            for i in range(3):
+                weight_handed(i, peer(k)).wait_recv()
+            return 0
+
+        lax.fori_loop(1, n, weights_ready, 0)
+        for i in range(3):
+            own_weights(i).wait()
 
         def project_rows(src):
-            xcopy(src, u, 1, s, u).wait_recv()
+            for m in range(half):
+                xcopy(src, u, 1, s, u, m).wait_recv()
             lhs = rows2[pl.ds(2 * src, 2)].reshape(tok, model)
             got = jnp.dot(lhs, weights[...], preferred_element_type=F32).astype(BF16)
             for i in range(3):
                 heads[i, trows(src, reach)] = got[:, i * head : (i + 1) * head]
 
-        def near_rows(k, _):
-            src = lax.rem(side + 2 * k, n)
-            xcopy(src, t, 0, side, t).wait_recv()
-            xcopy(src, t, 1, s, u).start()
-            project_rows(lax.rem(s + 2 * k, n))
-            return 0
-
-        lax.fori_loop(0, half, near_rows, 0)
-
-        def far_rows(k, _):
+        def far_rows(m, _):
+            for k in range(half):
+                src = lax.rem(side + 2 * k, n)
+                xcopy(src, t, 0, side, t, m).wait_recv()
+                xcopy(src, t, 1, s, u, m).start()
+            project_rows(peer(2 * m))
+            return 0
+
+        lax.fori_loop(0, half, far_rows, 0)
+
+        def last_rows(k, _):
             project_rows(lax.rem(side + 2 * k, n))
             return 0
 
-        lax.fori_loop(0, half, far_rows, 0)
-
-        values, drain2 = layer_branch(
-            1, mixed2, parts2, branch2, gs, gr, bs.at[1], br.at[1], lambda b: None
-        )
+        lax.fori_loop(0, half, last_rows, 0)
+
+        values, drain2 = layer_branch(1, mixed2, gs, gr, lambda b: None, lambda: None)
         done = (res[...].astype(F32) + scaled(values) * post2[...]).astype(BF16)
         last[t] = done
         final = rcopy(last.at[t], last.at[t], ys, yr, s, u)
@@ -444,17 +509,26 @@
 
         lax.fori_loop(0, n, lambda b, c: drain1(b, c), 0)
         lax.fori_loop(0, n, lambda b, c: drain2(b, c), 0)
-        for k in range(1, n):
+        def drain_first(k, _):
             for i in range(3):
                 head_copy(i, qkv[i], peer(k), s).wait_send()
-                weight_copy(i, wqkv[i], peer(k), s).wait_send()
-        for k in range(half + 1):
-            xcopy(s, t, k, side, t).wait_send()
-        for k in range(1, half):
-            xcopy(peer(2 * k), t, 0, side, t).wait_send()
-            xcopy(peer(2 * k), t, 1, side, t).wait_send()
-        for k in range(half):
-            xcopy(lax.rem(side + 2 * k, n), t, 1, side, t).wait_send()
+                weight_copy(i, peer(k), s).wait_send()
+                weight_hand(i, peer(k)).wait_send()
+            return 0
+
+        lax.fori_loop(1, n, drain_first, 0)
+
+        def drain_rows(m, _):
+            for k in range(half + 1):
+                xcopy(s, t, k, side, t, m).wait_send()
+            for k in range(1, half):
+                xcopy(peer(2 * k), t, 0, side, t, m).wait_send()
+                xcopy(peer(2 * k), t, 1, side, t, m).wait_send()
+            for k in range(half):
+                xcopy(lax.rem(side + 2 * k, n), t, 1, side, t, m).wait_send()
+            return 0
+
+        lax.fori_loop(0, half, drain_rows, 0)
         final.wait_send()
         rcopy(last.at[u], last.at[u], ys, yr, s, u).wait_recv()
         out_ref[:share] = last[0]
@@ -469,8 +543,8 @@
         pltpu.VMEM((2, tok, span), F32),
         pltpu.VMEM((n, n * tok, head), BF16),
         pltpu.VMEM((n, n * tok, head), BF16),
-        pltpu.VMEM((n, 2, share, cols), BF16),
-        pltpu.VMEM((n, 2, share, cols), BF16),
+        pltpu.VMEM((2, n, 2, share, cols), BF16),
+        pltpu.VMEM((2, n, share, cols), BF16),
         pltpu.VMEM((2, n, share, cols), BF16),
         pltpu.VMEM((2, n, share, cols), BF16),
         pltpu.VMEM((2 * n, share, width), BF16),
@@ -479,26 +553,22 @@
         pltpu.SemaphoreType.DMA((3, n)),
         pltpu.SemaphoreType.DMA((3, n)),
         pltpu.SemaphoreType.DMA((3, n)),
+        pltpu.SemaphoreType.DMA((3, n, 2)),
         pltpu.SemaphoreType.DMA((3, n)),
         pltpu.SemaphoreType.DMA((n, 2 * half - 1)),
         pltpu.SemaphoreType.DMA((n, n)),
         pltpu.SemaphoreType.DMA((n, 2 * half - 1)),
         pltpu.SemaphoreType.DMA((n, n)),
-        pltpu.SemaphoreType.DMA((2, n, 2)),
-        pltpu.SemaphoreType.DMA((2, 2, n)),
-        pltpu.SemaphoreType.DMA((n, half + 1)),
-        pltpu.SemaphoreType.DMA((2 * n,)),
+        pltpu.SemaphoreType.DMA((2, n)),
+        pltpu.SemaphoreType.DMA((2, n)),
+        pltpu.SemaphoreType.DMA((2, n)),
+        pltpu.SemaphoreType.DMA((2, n)),
+        pltpu.SemaphoreType.DMA((n, half + 1, half)),
+        pltpu.SemaphoreType.DMA((2 * n, half)),
         pltpu.SemaphoreType.DMA,
         pltpu.SemaphoreType.DMA,
     ]
     return kernel, scratch
-
-
-def reversed_line(table, tok):
-    top = table[:, -1:]
-    return jnp.concatenate(
-        [table[:, :0:-1], jnp.broadcast_to(top, (table.shape[0], tok))], axis=1
-    )
 
 
 def by_heads(
@@ -509,7 +579,7 @@
     tok, width = resid.shape
     head = queries_first.shape[1] // rel_first.shape[0]
     kernel, scratch = build_kernel(n, tok, head, width, REACH)
-    hbm = pl.BlockSpec(memory_space=pl.ANY)
+    hbm = pl.BlockSpec(memory_space=pltpu.HBM)
     vmem = pl.BlockSpec(memory_space=pltpu.VMEM)
     return pl.pallas_call(
         kernel,
@@ -518,11 +588,11 @@
         out_specs=vmem,
         scratch_shapes=scratch,
         compiler_params=pltpu.CompilerParams(
-            collective_id=0, has_side_effects=True, vmem_limit_bytes=40 * 2**20
+            collective_id=0, has_side_effects=True, vmem_limit_bytes=60 * 2**20
         ),
     )(
         queries_first, keys_first, values_first, query_weight, key_weight, value_weight, resid,
-        out_first, out_second, reversed_line(rel_first, tok), reversed_line(rel_second, tok),
+        out_first, out_second, rel_first, rel_second,
         post_first[None], pre_second[None], post_second[None],
     )
 

time: 201 us -> 146 us (0.73)
  Pallas kernels: 187 us -> 143 us
  local copies, waits for them, and re-layouts: 13.4 us -> 1.88 us
    pallas_call x1, Pallas kernels: 187 us -> 143 us  [by_heads(): pl.pallas_call(kernel, out_shape=jax.ShapeDtypeStruct((tok, width), BF16)...]
    unnamed x29 -> x1, local copies, waits for them, and re-layouts: 11.1 us -> 1.88 us
where the time goes in v2:
time: 146 us; the launch traced here: 145 us
  Pallas kernels  143 us (98%)
  local copies, waits for them, and re-layouts  1.88 us (1%)
    pallas_call x1, Pallas kernels, by_heads(): pl.pallas_call(kernel, out_shape=jax.ShapeDtypeStruct((tok, width), BF16)...  143 us

profile of v2, /device:TPU:29, one launch (start us, length us, event | category | flops | bytes accessed | tf_op | source)
XLA Modules:
  0.0 144.9 jit_solution(14872621442731833451)
XLA Ops:
  0.0 143.0 %shard_map.136 = bf16[128,2048]{1,0:T(8,128)(2,1)} custom-call(bf16[128,1024]{1,0:T(8,128)(2,1)} %q_hbm.1, bf16[128,1024]{1,0:T(8,128)(2,1)} %k_hbm.1, bf16[128,1024]{1,0:T(8,128)(2,1)} %v_hbm.1, bf16[256,1024]{1,0:T(8,128)(2,1)} %wq_hbm.1, bf16[256,1024]{1,0:T(8,128)(2,1)} %wk_hbm.1, bf16[256,1024]{1,0:T(8,128)(2,1)} %wv_hbm.1, ...), custom_call_target="tpu_custom_call" | custom-call | tf_op jit(solution)/shard_map/pallas_call | solution.py:584
  143.1 1.9 %copy.16 = bf16[128,2048]{1,0:T(8,128)(2,1)} copy(bf16[128,2048]{1,0:T(8,128)(2,1)} %shard_map.136) | data formatting | bytes 1048576

commit v3 on v2

--- a/solution.py
+++ b/solution.py
@@ -186,7 +186,7 @@
         q_hbm, k_hbm, v_hbm, wq_hbm, wk_hbm, wv_hbm, resid_hbm, o1_hbm, o2_hbm,
         rel1, rel2, post1, pre2, post2,
         out_ref,
-        heads, weights, outs, res, bias, mixed1, mixed2, parts, inbox, joined, branch, rows2, last,
+        heads, weights, outs, res, bias, mixed1, mixed2, parts, inbox, joined, branch, rows2, total, last,
         loc_sem, hs, hr, ws, wr, wf, fs, fr, gs, gr, ps, pr, bs, br, xs, xr, ys, yr,
     ):
         s = lax.axis_index("sp")
@@ -332,12 +332,22 @@
 
             half = n // 2
 
+            def forward(b):
+                for k in range(1, half):
+                    mcopy(b, peer(2 * k), k, side).wait_recv()
+                    mcopy(b, peer(2 * k), half - 1 + k, side).start()
+
             def own(b, _):
                 wait_block(b)
                 mixed[s, trows(b)] = attend(layer, b)
                 mcopy(b, s, 0, side).start()
                 for k in range(1, half):
                     mcopy(b, s, k, peer(2 * k)).start()
+
+                @pl.when(b >= half)
+                def _():
+                    forward(b - half)
+
                 return 0
 
             lax.fori_loop(0, n, own, 0)
@@ -354,11 +364,6 @@
                     joined.at[layer, b], branch.at[layer, src],
                     bs.at[layer, b], br.at[layer, src], b, t,
                 )
-
-            def forward(b):
-                for k in range(1, half):
-                    mcopy(b, peer(2 * k), k, side).wait_recv()
-                    mcopy(b, peer(2 * k), half - 1 + k, side).start()
 
             def project(b):
                 for k in range(half):
@@ -371,8 +376,8 @@
 
             def join(b):
                 pcopy(b).wait_recv()
-                total = parts[layer, b, t].astype(F32) + inbox[layer, b].astype(F32)
-                joined[layer, b] = total.astype(BF16)
+                both = parts[layer, b, t].astype(F32) + inbox[layer, b].astype(F32)
+                joined[layer, b] = both.astype(BF16)
 
                 @pl.when(b != s)
                 def _():
@@ -385,21 +390,19 @@
                     ).start()
 
             def step(b, _):
-                forward(b)
+                @pl.when(b < half)
+                def _():
+                    forward(n - half + b)
+
+                project(b)
 
                 @pl.when(b > 0)
                 def _():
-                    project(b - 1)
-
-                @pl.when(b > 1)
-                def _():
-                    join(b - 2)
+                    join(b - 1)
 
                 return 0
 
             lax.fori_loop(0, n, step, 0)
-            project(n - 1)
-            join(n - 2)
             join(n - 1)
 
             def arrived(j, _):
@@ -477,29 +480,31 @@
         for i in range(3):
             own_weights(i).wait()
 
-        def project_rows(src):
-            for m in range(half):
+        def project_rows(m):
+            for src in range(n):
                 xcopy(src, u, 1, s, u, m).wait_recv()
-            lhs = rows2[pl.ds(2 * src, 2)].reshape(tok, model)
-            got = jnp.dot(lhs, weights[...], preferred_element_type=F32).astype(BF16)
-            for i in range(3):
-                heads[i, trows(src, reach)] = got[:, i * head : (i + 1) * head]
+            depth = pl.ds(pl.multiple_of(m * wide, wide), wide)
+            lhs = rows2[:, :, depth].reshape(n * tok, wide)
+            total[...] += jnp.dot(lhs, weights[depth, :], preferred_element_type=F32)
+
+        total[...] = jnp.zeros_like(total)
 
         def far_rows(m, _):
             for k in range(half):
                 src = lax.rem(side + 2 * k, n)
                 xcopy(src, t, 0, side, t, m).wait_recv()
                 xcopy(src, t, 1, s, u, m).start()
-            project_rows(peer(2 * m))
+
+            @pl.when(m > 0)
+            def _():
+                project_rows(m - 1)
+
             return 0
 
         lax.fori_loop(0, half, far_rows, 0)
-
-        def last_rows(k, _):
-            project_rows(lax.rem(side + 2 * k, n))
-            return 0
-
-        lax.fori_loop(0, half, last_rows, 0)
+        project_rows(half - 1)
+        for i in range(3):
+            heads[i, reach:] = total[:, i * head : (i + 1) * head].astype(BF16)
 
         values, drain2 = layer_branch(1, mixed2, gs, gr, lambda b: None, lambda: None)
         done = (res[...].astype(F32) + scaled(values) * post2[...]).astype(BF16)
@@ -548,6 +553,7 @@
         pltpu.VMEM((2, n, share, cols), BF16),
         pltpu.VMEM((2, n, share, cols), BF16),
         pltpu.VMEM((2 * n, share, width), BF16),
+        pltpu.VMEM((n * tok, 3 * head), F32),
         pltpu.VMEM((2, share, width), BF16),
         pltpu.SemaphoreType.DMA((3,)),
         pltpu.SemaphoreType.DMA((3, n)),

time: 146 us -> 145 us (level)
  no operation moved by 1% of the time
where the time goes in v3:
time: 145 us
  Pallas kernels  143 us (99%)
  local copies, waits for them, and re-layouts  1.88 us (1%)
    pallas_call x1, Pallas kernels, by_heads(): pl.pallas_call(kernel, out_shape=jax.ShapeDtypeStruct((tok, width), BF16)...  143 us

profile of v3, /device:TPU:29, one launch (start us, length us, event | category | flops | bytes accessed | tf_op | source)
XLA Modules:
  0.0 144.6 jit_solution(12143424357266452576)
XLA Ops:
  0.0 142.7 %shard_map.136 = bf16[128,2048]{1,0:T(8,128)(2,1)} custom-call(bf16[128,1024]{1,0:T(8,128)(2,1)} %q_hbm.1, bf16[128,1024]{1,0:T(8,128)(2,1)} %k_hbm.1, bf16[128,1024]{1,0:T(8,128)(2,1)} %v_hbm.1, bf16[256,1024]{1,0:T(8,128)(2,1)} %wq_hbm.1, bf16[256,1024]{1,0:T(8,128)(2,1)} %wk_hbm.1, bf16[256,1024]{1,0:T(8,128)(2,1)} %wv_hbm.1, ...), custom_call_target="tpu_custom_call" | custom-call | tf_op jit(solution)/shard_map/pallas_call | solution.py:590
  142.7 1.9 %copy.16 = bf16[128,2048]{1,0:T(8,128)(2,1)} copy(bf16[128,2048]{1,0:T(8,128)(2,1)} %shard_map.136) | data formatting | bytes 1048576
